TPU v7x, 32 devices: a whole 2x2x4 slice. The times are simulated.
32 devices in a mesh: dp: 4 (over y, x), kv: 4 (over z), tp: 2 (over core).
Axes of the slice: x: 2, y: 2, z: 4, core: 2. Of those that a mesh axis runs over, the one named last changes fastest.
Arguments:
- tokens: bfloat16 [128, 2048], P('dp', ('kv', 'tp')), may hold values from -60 to 60
- first_norm_gain: float32 [2048], replicated, may hold values from 0.1 to 1.9
- first_gate_weight: bfloat16 [2048, 5632], P(None, ('kv', 'tp')), may hold values from -0.125 to 0.125
- first_up_weight: bfloat16 [2048, 5632], P(None, ('kv', 'tp')), may hold values from -0.125 to 0.125
- first_down_weight: bfloat16 [5632, 2048], P(('kv', 'tp')), may hold values from -0.109375 to 0.109375
- mixer_norm_gain: float32 [2048], replicated, may hold values from 0.1 to 1.9
- query_weight: bfloat16 [2048, 1024], P('kv', 'tp'), may hold values from -0.125 to 0.125
- key_weight: bfloat16 [2048, 1024], P('kv', 'tp'), may hold values from -0.125 to 0.125
- value_weight: bfloat16 [2048, 1024], P('kv', 'tp'), may hold values from -0.125 to 0.125
- output_gate_weight: bfloat16 [2048, 1024], P('kv', 'tp'), may hold values from -0.125 to 0.125
- strength_weight: bfloat16 [2048, 8], replicated, may hold values from -0.125 to 0.125
- decay_weight: bfloat16 [2048, 8], replicated, may hold values from -0.125 to 0.125
- head_decay_log: float32 [8], replicated, may hold values from 0 to 2.77
- decay_input_bias: float32 [8], replicated, may hold values from -4 to 0
- decay_extra_log: float32 [128, 8], P(('dp', 'kv'), 'tp'), may hold values from -0.7 to 0
- head_norm_gain: float32 [128], replicated, may hold values from 0.1 to 1.9
- state: float32 [128, 8, 128, 128], P(('dp', 'kv'), 'tp'), may hold values from -0.6 to 0.6
- mixer_output_weight: bfloat16 [1024, 2048], P('tp', 'kv'), may hold values from -0.1875 to 0.1875
- second_norm_gain: float32 [2048], replicated, may hold values from 0.1 to 1.9
- second_gate_weight: bfloat16 [2048, 5632], P(None, ('kv', 'tp')), may hold values from -0.125 to 0.125
- second_up_weight: bfloat16 [2048, 5632], P(None, ('kv', 'tp')), may hold values from -0.125 to 0.125
- second_down_weight: bfloat16 [5632, 2048], P(('kv', 'tp')), may hold values from -0.109375 to 0.109375
Outputs:
- layer_out: bfloat16 [128, 2048], P('dp', ('kv', 'tp'))
- new_state: float32 [128, 8, 128, 128], P(('dp', 'kv'), 'tp')
All inputs are finite; a program needn't handle non-finite values.
Results may differ from a plain program's by a relative error of at most 0.014.
Values may be sent and summed in bfloat16 or wider, within the bound.
A program may use at most 64 MiB of HBM per device.

v0:
```python
import jax
import jax.numpy as jnp
from jax import lax
from jax.sharding import PartitionSpec as P

EPS = 1e-06


def row_scale(values):
    return lax.rsqrt(jnp.mean(values * values, axis=-1, keepdims=True) + EPS)


def unit_rows(values):
    return values * lax.rsqrt(jnp.sum(values * values, axis=-1, keepdims=True) + EPS)


def block_terms(row_data, gain_vec, w_gate, w_up, w_down):
    rows32 = row_data.astype(jnp.float32)
    normed = (rows32 * row_scale(rows32) * gain_vec).astype(jnp.bfloat16)
    gate_pre = jnp.dot(normed, w_gate, preferred_element_type=jnp.float32)
    upward = jnp.dot(normed, w_up, preferred_element_type=jnp.float32)
    hidden = (jax.nn.silu(gate_pre) * upward).astype(jnp.bfloat16)
    return jnp.dot(hidden, w_down, preferred_element_type=jnp.float32)


def delta_step(
    query_vec, key_vec, value_vec, gate_vals, beta_gate, head_decay_rate, state, head_norm_gain
):
    recalled = jnp.einsum("shd,shde->she", key_vec, state, precision=lax.Precision.HIGHEST)
    correction = beta_gate[..., None] * (value_vec - head_decay_rate[..., None] * recalled)
    new_state = (
        head_decay_rate[..., None, None] * state + key_vec[..., :, None] * correction[..., None, :]
    )
    read_out = jnp.einsum("shd,shde->she", query_vec, new_state, precision=lax.Precision.HIGHEST)
    normed = read_out * row_scale(read_out) * head_norm_gain
    return (normed * jax.nn.silu(gate_vals), new_state)


def shards(
    tokens,
    first_norm_gain,
    first_gate_weight,
    first_up_weight,
    first_down_weight,
    mixer_norm_gain,
    query_weight,
    key_weight,
    value_weight,
    output_gate_weight,
    strength_weight,
    decay_weight,
    head_decay_log,
    decay_input_bias,
    decay_extra_log,
    head_norm_gain,
    state,
    mixer_output_weight,
    second_norm_gain,
    second_gate_weight,
    second_up_weight,
    second_down_weight,
):
    batch_rows, columns = tokens.shape
    kv_index = lax.axis_index("kv")
    tp_index = lax.axis_index("tp")
    own_block = kv_index * lax.axis_size("tp") + tp_index
    seq_dev, heads_dev, head_size = (state.shape[0], state.shape[1], state.shape[2])
    kv_width = query_weight.shape[0]
    head_cols = heads_dev * head_size
    model_width = mixer_norm_gain.shape[0]
    rows_all = lax.all_gather(tokens, ("kv", "tp"), axis=1, tiled=True)
    ffn_terms = block_terms(
        rows_all, first_norm_gain, first_gate_weight, first_up_weight, first_down_weight
    )
    share_sum = lax.psum_scatter(
        ffn_terms.astype(jnp.bfloat16), ("kv", "tp"), scatter_dimension=1, tiled=True
    ).astype(jnp.float32)
    first_rows = (tokens.astype(jnp.float32) + 0.5 * share_sum).astype(jnp.bfloat16)
    first32 = first_rows.astype(jnp.float32)
    kv_block = lax.all_gather(first_rows, "tp", axis=1, tiled=True)
    own_gain = lax.dynamic_slice_in_dim(mixer_norm_gain, own_block * columns, columns)
    own_scaled = (first32 * own_gain).astype(jnp.bfloat16)
    beta_rows = lax.dynamic_slice_in_dim(strength_weight, own_block * columns, columns, 0)
    decay_rows = lax.dynamic_slice_in_dim(decay_weight, own_block * columns, columns, 0)
    squares, beta_pre, decay_logits = lax.psum(
        (
            jnp.sum(first32 * first32, axis=1),
            jnp.dot(own_scaled, beta_rows, preferred_element_type=jnp.float32),
            jnp.dot(own_scaled, decay_rows, preferred_element_type=jnp.float32),
        ),
        ("kv", "tp"),
    )
    row_factor = lax.rsqrt(squares / model_width + EPS)
    block_gain = lax.dynamic_slice_in_dim(mixer_norm_gain, kv_index * kv_width, kv_width)
    block_scaled = (kv_block.astype(jnp.float32) * block_gain).astype(jnp.bfloat16)
    projected = lax.psum_scatter(
        jnp.concatenate(
            [
                jnp.dot(block_scaled, weight, preferred_element_type=jnp.float32)
                for weight in (query_weight, key_weight, value_weight, output_gate_weight)
            ],
            axis=1,
        ).astype(jnp.bfloat16),
        "kv",
        scatter_dimension=0,
        tiled=True,
    ).astype(jnp.float32)
    own_rows = kv_index * seq_dev
    own_factor = lax.dynamic_slice_in_dim(row_factor, own_rows, seq_dev)[:, None]
    projected = projected * own_factor

    def split_heads(role_index):
        return projected[:, role_index * head_cols : (role_index + 1) * head_cols].reshape(
            seq_dev, heads_dev, head_size
        )

    query_vec = unit_rows(jax.nn.silu(split_heads(0))) * head_size ** (-0.5)
    key_vec = unit_rows(jax.nn.silu(split_heads(1)))
    value_vec = jax.nn.silu(split_heads(2))
    gate_vals = split_heads(3)
    head_start = tp_index * heads_dev

    def local_gate_values(values):
        own_seqs = lax.dynamic_slice_in_dim(values, own_rows, seq_dev, 0)
        return lax.dynamic_slice_in_dim(own_seqs, head_start, heads_dev, 1) * own_factor

    beta_gate = jax.nn.sigmoid(local_gate_values(beta_pre))
    decay_log_term = lax.dynamic_slice_in_dim(head_decay_log, head_start, heads_dev)
    decay_offset_term = lax.dynamic_slice_in_dim(decay_input_bias, head_start, heads_dev)
    head_decay_rate = jnp.exp(
        decay_extra_log
        - jnp.exp(decay_log_term)
        * jax.nn.softplus(local_gate_values(decay_logits) + decay_offset_term)
    )
    heads_f32, new_state = delta_step(
        query_vec, key_vec, value_vec, gate_vals, beta_gate, head_decay_rate, state, head_norm_gain
    )
    heads_out = heads_f32.reshape(seq_dev, head_cols).astype(jnp.bfloat16)
    mixer_terms = jnp.dot(
        lax.all_gather(heads_out, "kv", axis=0, tiled=True),
        mixer_output_weight,
        preferred_element_type=jnp.float32,
    )
    mixer_sum = lax.psum_scatter(
        mixer_terms.astype(jnp.bfloat16), "tp", scatter_dimension=1, tiled=True
    ).astype(jnp.float32)
    second_rows = (first32 + mixer_sum).astype(jnp.bfloat16)
    rows_last = lax.all_gather(second_rows, ("kv", "tp"), axis=1, tiled=True)
    last_terms = block_terms(
        rows_last, second_norm_gain, second_gate_weight, second_up_weight, second_down_weight
    )
    last_sum = lax.psum_scatter(
        last_terms.astype(jnp.bfloat16), ("kv", "tp"), scatter_dimension=1, tiled=True
    ).astype(jnp.float32)
    layer_out = (second_rows.astype(jnp.float32) + 0.5 * last_sum).astype(jnp.bfloat16)
    return (layer_out, new_state)


def solution(mesh):
    placed = (
        P("dp", ("kv", "tp")),
        P(),
        P(None, ("kv", "tp")),
        P(None, ("kv", "tp")),
        P(("kv", "tp"), None),
        P(),
        P("kv", "tp"),
        P("kv", "tp"),
        P("kv", "tp"),
        P("kv", "tp"),
        P(),
        P(),
        P(),
        P(),
        P(("dp", "kv"), "tp"),
        P(),
        P(("dp", "kv"), "tp", None, None),
        P("tp", "kv"),
        P(),
        P(None, ("kv", "tp")),
        P(None, ("kv", "tp")),
        P(("kv", "tp"), None),
    )
    return jax.shard_map(
        shards,
        mesh=mesh,
        in_specs=placed,
        out_specs=(P("dp", ("kv", "tp")), P(("dp", "kv"), "tp", None, None)),
        check_vma=False,
    )
```

profile of v0, /device:TPU:0, one launch (start us, length us, event | category | flops | bytes accessed | tf_op | source)
XLA Modules:
  0.0 181.2 jit_solution(4792796293112144642)
XLA Ops:
  7.2 16.1 %all_gather.12 = bf16[32,2048]{1,0:T(8,128)(2,1)S(1)} all-gather(bf16[32,256]{1,0:T(8,128)(2,1)} %param.22), channel_id=1, replica_groups=mesh['dp'=4,'kv'=4,'tp'=2] {'kv','tp'}, dimensions={1}, use_global_device_ids=true | all-gather | bytes 147456 | tf_op jit(solution)/shard_map/all_gather | solution.py:71
  24.0 3.4 %fusion.26 = f32[32,704]{1,0:T(8,128)} fusion(bf16[2048,704]{0,1:T(8,128)(2,1)} %param.24, bf16[32,2048]{1,0:T(8,128)(2,1)S(1)} %all_gather.12, f32[2048]{0:T(1024)} %param.23, f32[32]{0:T(128)S(1)} %add_rsqrt_fusion.5), kind=kOutput, calls=%fused_computation.41 | convolution fusion | flops 92536832 | bytes 3113088 | tf_op jit(solution)/shard_map/dot_general | solution.py:20
  27.4 4.3 %convolution_convert_fusion.1 = bf16[32,2048]{1,0:T(8,128)(2,1)} fusion(bf16[704,2048]{1,0:T(8,128)(2,1)S(1)} %copy-done, bf16[2048,704]{0,1:T(8,128)(2,1)} %param.25, f32[32,704]{1,0:T(8,128)} %fusion.26, bf16[32,2048]{1,0:T(8,128)(2,1)S(1)} %all_gather.12, f32[2048]{0:T(1024)} %param.23, f32[32]{0:T(128)} %copy-done.8), kind=kOutput, calls=%fused_computation.1 | convolution fusion | flops 185012224 | bytes 6127744 | tf_op jit(solution)/shard_map/dot_general | solution.py:23
  34.8 28.7 %reduce-scatter.5.cloned.1.call-done = bf16[32,256]{1,0:T(8,128)(2,1)} async-done(((bf16[32,2048]{1,0:T(8,128)(2,1)}), bf16[32,256]{1,0:T(8,128)(2,1)}) %reduce-scatter.5.cloned.1.call-update) | async-done | bytes 16400 | tf_op jit(solution)/shard_map/reduce_scatter | solution.py:75
  63.5 0.8 fusion.28
  64.3 1.8 %all_gather.13 = bf16[32,512]{1,0:T(8,128)(2,1)S(1)} all-gather(bf16[32,256]{1,0:T(8,128)(2,1)S(1)} %get-tuple-element.8), channel_id=1, replica_groups=mesh['dp'=4,'kv'=4,'tp'=2] {'tp'}, dimensions={1}, use_global_device_ids=true | all-gather | bytes 49152 | tf_op jit(solution)/shard_map/all_gather | solution.py:80
  66.2 0.8 fusion.43
  67.0 0.8 fusion.41
  68.0 1.2 convolution_convert_fusion.4
  69.2 1.2 convolution_convert_fusion.3
  70.5 1.3 convolution_convert_fusion.6
  72.5 14.4 %all-reduce = (f32[32]{0:T(128)S(1)}, f32[32,8]{0,1:T(8,128)S(1)}, f32[32,8]{0,1:T(8,128)S(1)}) all-reduce(f32[32]{0:T(128)S(1)} %get-tuple-element.7, f32[32,8]{0,1:T(8,128)S(1)} %fusion.43, f32[32,8]{0,1:T(8,128)S(1)} %fusion.41), channel_id=1, replica_groups=mesh['dp'=4,'kv'=4,'tp'=2] {'kv','tp'}, use_global_device_ids=true, to_apply=%region_4.5 | all-reduce | flops 544 | bytes 4352 | tf_op jit(solution)/shard_map/psum | solution.py:85
  87.1 3.0 %reduce-scatter.7.cloned.1.call-done = bf16[8,2048]{1,0:T(8,128)(2,1)} async-done(((bf16[32,2048]{1,0:T(8,128)(2,1)}), bf16[8,2048]{1,0:T(8,128)(2,1)}) %reduce-scatter.7.cloned.1.call-update) | async-done | bytes 32784 | tf_op jit(solution)/shard_map/reduce_scatter | solution.py:96
  90.1 1.0 convert_multiply_fusion.4
  91.4 3.4 %fusion.39 = f32[8,4,1,128]{3,2,1,0:T(1,128)S(1)} fusion(f32[8,4,128,128]{3,2,1,0:T(8,128)} %param.38, f32[8,4,128,1]{2,0,1,3:T(8,128)S(1)} %fusion.69), kind=kOutput, calls=%fused_computation.62 | convolution fusion | flops 6291456 | bytes 2129920 | tf_op jit(solution)/shard_map/shd,shde->she/dot_general | solution.py:29
  95.7 1.3 copy-done.2
  97.0 1.9 %fusion.37 = f32[8,4,1,128]{3,2,1,0:T(1,128)S(1)} fusion(f32[8,4,128,128]{3,2,1,0:T(8,128)S(1)} %multiply_add_fusion, f32[8,4,128,1]{2,0,1,3:T(8,128)S(1)} %get-tuple-element.9), kind=kOutput, calls=%fused_computation.60 | convolution fusion | flops 6291456 | bytes 2129920 | tf_op jit(solution)/shard_map/shd,shde->she/dot_general | solution.py:34
  99.1 13.1 %all_gather.14 = bf16[32,512]{1,0:T(8,128)(2,1)S(1)} all-gather(bf16[8,512]{1,0:T(8,128)(2,1)S(1)} %fusion.45), channel_id=1, replica_groups=mesh['dp'=4,'kv'=4,'tp'=2] {'kv'}, dimensions={0}, use_global_device_ids=true | all-gather | bytes 40960 | tf_op jit(solution)/shard_map/all_gather | solution.py:140
  113.1 5.8 %reduce-scatter.9.cloned.1.call-done = bf16[32,256]{1,0:T(8,128)(2,1)} async-done(((bf16[32,512]{1,0:T(8,128)(2,1)}), bf16[32,256]{1,0:T(8,128)(2,1)}) %reduce-scatter.9.cloned.1.call-update) | async-done | bytes 16400 | tf_op jit(solution)/shard_map/reduce_scatter | solution.py:144
  119.6 14.3 %all_gather.15 = bf16[32,2048]{1,0:T(8,128)(2,1)S(1)} all-gather(bf16[32,256]{1,0:T(8,128)(2,1)S(1)} %fusion.30), channel_id=1, replica_groups=mesh['dp'=4,'kv'=4,'tp'=2] {'kv','tp'}, dimensions={1}, use_global_device_ids=true | all-gather | bytes 147456 | tf_op jit(solution)/shard_map/all_gather | solution.py:148
  134.0 2.7 %fusion.22 = f32[32,704]{1,0:T(8,128)S(1)} fusion(bf16[2048,704]{0,1:T(8,128)(2,1)} %param.41, bf16[32,2048]{1,0:T(8,128)(2,1)S(1)} %all_gather.15, f32[2048]{0:T(1024)S(1)} %copy-done.6, f32[32]{0:T(128)S(1)} %add_rsqrt_fusion.3), kind=kOutput, calls=%fused_computation.40 | convolution fusion | flops 92536832 | bytes 3113088 | tf_op jit(solution)/shard_map/dot_general | solution.py:20
  136.7 5.1 %convolution_convert_fusion = bf16[32,2048]{1,0:T(8,128)(2,1)} fusion(bf16[704,2048]{1,0:T(8,128)(2,1)} %param.43, bf16[2048,704]{0,1:T(8,128)(2,1)} %param.42, f32[32,704]{1,0:T(8,128)S(1)} %fusion.22, bf16[32,2048]{1,0:T(8,128)(2,1)S(1)} %all_gather.15, f32[2048]{0:T(1024)S(1)} %copy-done.6, f32[32]{0:T(128)S(1)} %add_rsqrt_fusion.3), kind=kOutput, calls=%fused_computation | convolution fusion | flops 185012224 | bytes 6127744 | tf_op jit(solution)/shard_map/dot_general | solution.py:23
  141.9 31.5 %reduce-scatter.11.cloned.1.call-done = bf16[32,256]{1,0:T(8,128)(2,1)} async-done(((bf16[32,2048]{1,0:T(8,128)(2,1)}), bf16[32,256]{1,0:T(8,128)(2,1)}) %reduce-scatter.11.cloned.1.call-update) | async-done | bytes 16400 | tf_op jit(solution)/shard_map/reduce_scatter | solution.py:152
  173.4 1.3 add_convert_fusion
  (54 shorter events, 8.0 us)
Async XLA Ops:
  7.2 20.2 %copy-start = (bf16[704,2048]{1,0:T(8,128)(2,1)S(1)}, bf16[704,2048]{1,0:T(8,128)(2,1)}, u32[]{:S(2)}) copy-start(bf16[704,2048]{1,0:T(8,128)(2,1)} %param.26) | copy-start | bytes 8650756
  7.2 56.3 %reduce-scatter.5.cloned.1.call-start = ((), (), s32[]{:S(2)}) async-start(), calls=%async_computation.4 | async-start | bytes 147456 | tf_op jit(solution)/shard_map/reduce_scatter | solution.py:75
  23.5 0.5 copy-start.8
  27.4 36.2 %copy-start.5 = (bf16[32,256]{1,0:T(8,128)(2,1)S(1)}, bf16[32,256]{1,0:T(8,128)(2,1)}, u32[]{:S(2)}) copy-start(bf16[32,256]{1,0:T(8,128)(2,1)} %param.22) | copy-start | bytes 49156
  27.4 40.4 %copy-start.3 = (bf16[512,512]{1,0:T(8,128)(2,1)S(1)}, bf16[512,512]{1,0:T(8,128)(2,1)}, u32[]{:S(2)}) copy-start(bf16[512,512]{1,0:T(8,128)(2,1)} %param.29) | copy-start | bytes 1572868
  31.7 55.2 %copy-start.7 = (f32[8,4]{0,1:T(4,128)S(1)}, f32[8,4]{0,1:T(4,128)}, u32[]{:S(2)}) copy-start(f32[8,4]{0,1:T(4,128)} %param.36) | copy-start | bytes 388
  31.7 58.4 %reduce-scatter.7.cloned.1.call-start = ((), (), s32[]{:S(2)}) async-start(), calls=%async_computation.5 | async-start | bytes 163840 | tf_op jit(solution)/shard_map/reduce_scatter | solution.py:96
  72.4 46.4 %reduce-scatter.9.cloned.1.call-start = ((), (), s32[]{:S(2)}) async-start(), calls=%async_computation.6 | async-start | bytes 49152 | tf_op jit(solution)/shard_map/reduce_scatter | solution.py:144
  90.1 4.8 %copy-start.1 = (f32[8,4,128,128]{3,2,1,0:T(8,128)S(1)}, f32[8,4,128,128]{3,2,1,0:T(8,128)}, u32[]{:S(2)}) copy-start(f32[8,4,128,128]{3,2,1,0:T(8,128)} %param.38) | copy-start | bytes 6291460
  94.9 4.1 %copy-start.9 = (f32[128]{0:T(128)S(1)}, f32[128]{0:T(128)}, u32[]{:S(2)}) copy-start(f32[128]{0:T(128)} %param.37) | copy-start | bytes 1540
  94.9 17.3 %copy-start.4 = (bf16[512,512]{1,0:T(8,128)(2,1)S(1)}, bf16[512,512]{1,0:T(8,128)(2,1)}, u32[]{:S(2)}) copy-start(bf16[512,512]{1,0:T(8,128)(2,1)} %param.39) | copy-start | bytes 1572868
  94.9 39.1 %copy-start.6 = (f32[2048]{0:T(1024)S(1)}, f32[2048]{0:T(1024)}, u32[]{:S(2)}) copy-start(f32[2048]{0:T(1024)} %param.40) | copy-start | bytes 24580
  95.7 1.3 copy-start.2
  113.0 60.3 %reduce-scatter.11.cloned.1.call-start = ((), (), s32[]{:S(2)}) async-start(), calls=%async_computation.7 | async-start | bytes 147456 | tf_op jit(solution)/shard_map/reduce_scatter | solution.py:152
Sparse Core Ops, SparseCore 0:
  31.8 31.6 reduce-scatter.4
  72.5 17.5 reduce-scatter.6
  113.2 5.6 reduce-scatter.8
  142.0 31.3 reduce-scatter.10
where the time goes:
time: 182 us; the launch traced here: 181 us
  waiting for transfers between devices  69.1 us (38%)
  blocking collectives  59.7 us (33%)
  matrix products  27.2 us (15%)
  between operations  13.9 us (8%)
  other arithmetic  6.18 us (3%)
  local copies, waits for them, and re-layouts  5.02 us (3%)
    reduce_scatter x1, waiting for transfers between devices, shards(): lax.psum_scatter(last_terms.astype(jnp.bfloat16), ('kv', 'tp'), scatter_d...  31.5 us
    reduce_scatter x1, waiting for transfers between devices, shards(): lax.psum_scatter(ffn_terms.astype(jnp.bfloat16), ('kv', 'tp'), scatter_di...  28.7 us
    all_gather x1, blocking collectives, shards(): rows_all = lax.all_gather(tokens, ('kv', 'tp'), axis=1, tiled=True)  16.1 us
    psum x1, blocking collectives, shards(): lax.psum((jnp.sum(first32 * first32, axis=1), jnp.dot(own_scaled, beta_ro...  14.4 us
    all_gather x1, blocking collectives, shards(): rows_last = lax.all_gather(second_rows, ('kv', 'tp'), axis=1, tiled=True)  14.3 us
    all_gather x1, blocking collectives, shards(): lax.all_gather(heads_out, 'kv', axis=0, tiled=True)  13.1 us
    dot_general x2, matrix products, block_terms(): return jnp.dot(hidden, w_down, preferred_element_type=jnp.float32)  9.45 us
    dot_general x2, matrix products, block_terms(): gate_pre = jnp.dot(normed, w_gate, preferred_element_type=jnp.float32)  6.1 us
  transfers between devices with their start and end apart: 4, of which 4 were waited for; matrix products, arithmetic and copies ran while one was open for 2% of the time, Pallas kernels for 0%

commit v1 on v0

--- a/solution.py
+++ b/solution.py
@@ -68,7 +68,8 @@
     kv_width = query_weight.shape[0]
     head_cols = heads_dev * head_size
     model_width = mixer_norm_gain.shape[0]
-    rows_all = lax.all_gather(tokens, ("kv", "tp"), axis=1, tiled=True)
+    parts = lax.all_gather(tokens, ("kv", "tp"), axis=0, tiled=False)
+    rows_all = jnp.concatenate(parts, axis=1)
     ffn_terms = block_terms(
         rows_all, first_norm_gain, first_gate_weight, first_up_weight, first_down_weight
     )

time: 182 us -> 182 us (level)
  transfers between devices with their start and end apart: 4 -> 4, of which waited for: 4 -> 4; matrix products, arithmetic and copies ran while one was open for 2% -> 1% of each run, Pallas kernels for 0% -> 0%
where the time goes in v1:
time: 182 us; the launch traced here: 181 us
  waiting for transfers between devices  70.5 us (39%)
  blocking collectives  59.7 us (33%)
  matrix products  27.5 us (15%)
  between operations  14 us (8%)
  other arithmetic  6.2 us (3%)
  local copies, waits for them, and re-layouts  3.26 us (2%)
    reduce_scatter x1, waiting for transfers between devices, shards(): lax.psum_scatter(last_terms.astype(jnp.bfloat16), ('kv', 'tp'), scatter_d...  31.6 us
    reduce_scatter x1, waiting for transfers between devices, shards(): lax.psum_scatter(ffn_terms.astype(jnp.bfloat16), ('kv', 'tp'), scatter_di...  30 us
    all_gather x1, blocking collectives, shards(): parts = lax.all_gather(tokens, ('kv', 'tp'), axis=0, tiled=False)  16.1 us
    psum x1, blocking collectives, shards(): lax.psum((jnp.sum(first32 * first32, axis=1), jnp.dot(own_scaled, beta_ro...  14.5 us
    all_gather x1, blocking collectives, shards(): rows_last = lax.all_gather(second_rows, ('kv', 'tp'), axis=1, tiled=True)  14.2 us
    all_gather x1, blocking collectives, shards(): lax.all_gather(heads_out, 'kv', axis=0, tiled=True)  13.1 us
    dot_general x2, matrix products, block_terms(): return jnp.dot(hidden, w_down, preferred_element_type=jnp.float32)  9.37 us
    reduce_scatter x1, waiting for transfers between devices, shards(): lax.psum_scatter(mixer_terms.astype(jnp.bfloat16), 'tp', scatter_dimensio...  5.75 us
  transfers between devices with their start and end apart: 4, of which 4 were waited for; matrix products, arithmetic and copies ran while one was open for 1% of the time, Pallas kernels for 0%

profile of v1, /device:TPU:0, one launch (start us, length us, event | category | flops | bytes accessed | tf_op | source)
XLA Modules:
  0.0 181.3 jit_solution(7438528477165620359)
XLA Ops:
  7.2 16.1 %all-gather = bf16[256,256]{1,0:T(8,128)(2,1)S(1)} all-gather(bf16[32,256]{1,0:T(8,128)(2,1)} %param.22), channel_id=2, replica_groups=mesh['dp'=4,'kv'=4,'tp'=2] {'kv','tp'}, dimensions={0}, use_global_device_ids=true | all-gather | bytes 147456 | tf_op jit(solution)/shard_map/all_gather | solution.py:71
  23.5 2.7 %fusion.48 = f32[32,704]{1,0:T(8,128)S(1)} fusion(bf16[2048,704]{0,1:T(8,128)(2,1)} %param.24, f32[32,2048]{1,0:T(8,128)S(1)} %bitcast.77, f32[2048]{0:T(1024)} %param.23, f32[32]{0:T(128)S(1)} %add_rsqrt_fusion.5), kind=kOutput, calls=%fused_computation.88 | convolution fusion | flops 92471296 | bytes 3244160 | tf_op jit(solution)/shard_map/dot_general | solution.py:20
  26.3 4.3 %convolution_convert_fusion.1 = bf16[32,2048]{1,0:T(8,128)(2,1)} fusion(bf16[704,2048]{1,0:T(8,128)(2,1)S(1)} %copy-done, bf16[2048,704]{0,1:T(8,128)(2,1)} %param.25, f32[32,704]{1,0:T(8,128)S(1)} %fusion.48, f32[32,2048]{1,0:T(8,128)S(1)} %bitcast.78, f32[2048]{0:T(1024)S(1)} %copy-done.5, f32[32]{0:T(128)S(1)} %add_rsqrt_fusion.5), kind=kOutput, calls=%fused_computation.1 | convolution fusion | flops 184946688 | bytes 6258816 | tf_op jit(solution)/shard_map/dot_general | solution.py:23
  32.4 30.0 %reduce-scatter.5.cloned.1.call-done = bf16[32,256]{1,0:T(8,128)(2,1)} async-done(((bf16[32,2048]{1,0:T(8,128)(2,1)}), bf16[32,256]{1,0:T(8,128)(2,1)}) %reduce-scatter.5.cloned.1.call-update) | async-done | bytes 16400 | tf_op jit(solution)/shard_map/reduce_scatter | solution.py:76
  62.4 0.8 fusion.21
  63.2 1.8 %all_gather.17 = bf16[32,512]{1,0:T(8,128)(2,1)S(1)} all-gather(bf16[32,256]{1,0:T(8,128)(2,1)S(1)} %get-tuple-element.8), channel_id=1, replica_groups=mesh['dp'=4,'kv'=4,'tp'=2] {'tp'}, dimensions={1}, use_global_device_ids=true | all-gather | bytes 49152 | tf_op jit(solution)/shard_map/all_gather | solution.py:81
  65.8 0.8 fusion.34
  66.7 1.2 convolution_convert_fusion.5
  67.9 1.2 convolution_convert_fusion.4
  69.1 1.2 convolution_convert_fusion.3
  70.4 1.3 convolution_convert_fusion.6
  72.4 14.5 %all-reduce = (f32[32]{0:T(128)S(1)}, f32[32,8]{0,1:T(8,128)S(1)}, f32[32,8]{0,1:T(8,128)S(1)}) all-reduce(f32[32]{0:T(128)S(1)} %get-tuple-element.7, f32[32,8]{0,1:T(8,128)S(1)} %fusion.36, f32[32,8]{0,1:T(8,128)S(1)} %fusion.34), channel_id=1, replica_groups=mesh['dp'=4,'kv'=4,'tp'=2] {'kv','tp'}, use_global_device_ids=true, to_apply=%region_4.5 | all-reduce | flops 544 | bytes 4352 | tf_op jit(solution)/shard_map/psum | solution.py:86
  87.1 3.0 %reduce-scatter.7.cloned.1.call-done = bf16[8,2048]{1,0:T(8,128)(2,1)} async-done(((bf16[32,2048]{1,0:T(8,128)(2,1)}), bf16[8,2048]{1,0:T(8,128)(2,1)}) %reduce-scatter.7.cloned.1.call-update) | async-done | bytes 32784 | tf_op jit(solution)/shard_map/reduce_scatter | solution.py:97
  90.1 1.0 convert_multiply_fusion.2
  91.4 3.4 %fusion.32 = f32[8,4,1,128]{3,2,1,0:T(1,128)S(1)} fusion(f32[8,4,128,128]{3,2,1,0:T(8,128)} %param.38, f32[8,4,128,1]{2,0,1,3:T(8,128)S(1)} %fusion.64), kind=kOutput, calls=%fused_computation.58 | convolution fusion | flops 6291456 | bytes 2129920 | tf_op jit(solution)/shard_map/shd,shde->she/dot_general | solution.py:29
  95.7 1.3 copy-done.2
  97.0 1.9 %fusion.30 = f32[8,4,1,128]{3,2,1,0:T(1,128)S(1)} fusion(f32[8,4,128,128]{3,2,1,0:T(8,128)S(1)} %multiply_add_fusion, f32[8,4,128,1]{2,0,1,3:T(8,128)S(1)} %get-tuple-element.9), kind=kOutput, calls=%fused_computation.56 | convolution fusion | flops 6291456 | bytes 2129920 | tf_op jit(solution)/shard_map/shd,shde->she/dot_general | solution.py:34
  99.1 13.1 %all_gather.18 = bf16[32,512]{1,0:T(8,128)(2,1)S(1)} all-gather(bf16[8,512]{1,0:T(8,128)(2,1)S(1)} %fusion.38), channel_id=1, replica_groups=mesh['dp'=4,'kv'=4,'tp'=2] {'kv'}, dimensions={0}, use_global_device_ids=true | all-gather | bytes 40960 | tf_op jit(solution)/shard_map/all_gather | solution.py:141
  113.1 5.8 %reduce-scatter.9.cloned.1.call-done = bf16[32,256]{1,0:T(8,128)(2,1)} async-done(((bf16[32,512]{1,0:T(8,128)(2,1)}), bf16[32,256]{1,0:T(8,128)(2,1)}) %reduce-scatter.9.cloned.1.call-update) | async-done | bytes 16400 | tf_op jit(solution)/shard_map/reduce_scatter | solution.py:145
  119.5 14.2 %all_gather.19 = bf16[32,2048]{1,0:T(8,128)(2,1)S(1)} all-gather(bf16[32,256]{1,0:T(8,128)(2,1)S(1)} %fusion.23), channel_id=1, replica_groups=mesh['dp'=4,'kv'=4,'tp'=2] {'kv','tp'}, dimensions={1}, use_global_device_ids=true | all-gather | bytes 147456 | tf_op jit(solution)/shard_map/all_gather | solution.py:149
  133.9 2.7 %fusion.19 = f32[32,704]{1,0:T(8,128)S(1)} fusion(bf16[2048,704]{0,1:T(8,128)(2,1)} %param.41, bf16[32,2048]{1,0:T(8,128)(2,1)S(1)} %all_gather.19, f32[2048]{0:T(1024)S(1)} %copy-done.6, f32[32]{0:T(128)S(1)} %add_rsqrt_fusion.3), kind=kOutput, calls=%fused_computation.37 | convolution fusion | flops 92536832 | bytes 3113088 | tf_op jit(solution)/shard_map/dot_general | solution.py:20
  136.6 5.1 %convolution_convert_fusion = bf16[32,2048]{1,0:T(8,128)(2,1)} fusion(bf16[704,2048]{1,0:T(8,128)(2,1)} %param.43, bf16[2048,704]{0,1:T(8,128)(2,1)} %param.42, f32[32,704]{1,0:T(8,128)S(1)} %fusion.19, bf16[32,2048]{1,0:T(8,128)(2,1)S(1)} %all_gather.19, f32[2048]{0:T(1024)S(1)} %copy-done.6, f32[32]{0:T(128)S(1)} %add_rsqrt_fusion.3), kind=kOutput, calls=%fused_computation | convolution fusion | flops 185012224 | bytes 6127744 | tf_op jit(solution)/shard_map/dot_general | solution.py:23
  141.8 31.6 %reduce-scatter.11.cloned.1.call-done = bf16[32,256]{1,0:T(8,128)(2,1)} async-done(((bf16[32,2048]{1,0:T(8,128)(2,1)}), bf16[32,256]{1,0:T(8,128)(2,1)}) %reduce-scatter.11.cloned.1.call-update) | async-done | bytes 16400 | tf_op jit(solution)/shard_map/reduce_scatter | solution.py:153
  173.4 1.3 add_convert_fusion
  (58 shorter events, 6.8 us)
Async XLA Ops:
  7.2 19.1 %copy-start = (bf16[704,2048]{1,0:T(8,128)(2,1)S(1)}, bf16[704,2048]{1,0:T(8,128)(2,1)}, u32[]{:S(2)}) copy-start(bf16[704,2048]{1,0:T(8,128)(2,1)} %param.26) | copy-start | bytes 8650756
  7.2 19.1 %copy-start.5 = (f32[2048]{0:T(1024)S(1)}, f32[2048]{0:T(1024)}, u32[]{:S(2)}) copy-start(f32[2048]{0:T(1024)} %param.23) | copy-start | bytes 24580
  7.2 55.2 %reduce-scatter.5.cloned.1.call-start = ((), (), s32[]{:S(2)}) async-start(), calls=%async_computation.4 | async-start | bytes 147456 | tf_op jit(solution)/shard_map/reduce_scatter | solution.py:76
  26.3 4.4 %copy-start.9 = (f32[8]{0:T(128)S(1)}, f32[8]{0:T(128)}, u32[]{:S(2)}) copy-start(f32[8]{0:T(128)} %param.35) | copy-start | bytes 100
  26.3 6.0 %copy-start.10 = (f32[8]{0:T(128)S(1)}, f32[8]{0:T(128)}, u32[]{:S(2)}) copy-start(f32[8]{0:T(128)} %param.34) | copy-start | bytes 100
  26.3 36.1 %copy-start.4 = (bf16[32,256]{1,0:T(8,128)(2,1)S(1)}, bf16[32,256]{1,0:T(8,128)(2,1)}, u32[]{:S(2)}) copy-start(bf16[32,256]{1,0:T(8,128)(2,1)} %param.22) | copy-start | bytes 49156
  30.6 56.3 %copy-start.7 = (f32[8,4]{0,1:T(4,128)S(1)}, f32[8,4]{0,1:T(4,128)}, u32[]{:S(2)}) copy-start(f32[8,4]{0,1:T(4,128)} %param.36) | copy-start | bytes 388
  30.6 59.5 %reduce-scatter.7.cloned.1.call-start = ((), (), s32[]{:S(2)}) async-start(), calls=%async_computation.5 | async-start | bytes 163840 | tf_op jit(solution)/shard_map/reduce_scatter | solution.py:97
  72.3 46.5 %reduce-scatter.9.cloned.1.call-start = ((), (), s32[]{:S(2)}) async-start(), calls=%async_computation.6 | async-start | bytes 49152 | tf_op jit(solution)/shard_map/reduce_scatter | solution.py:145
  90.1 4.8 %copy-start.1 = (f32[8,4,128,128]{3,2,1,0:T(8,128)S(1)}, f32[8,4,128,128]{3,2,1,0:T(8,128)}, u32[]{:S(2)}) copy-start(f32[8,4,128,128]{3,2,1,0:T(8,128)} %param.38) | copy-start | bytes 6291460
  94.9 4.1 %copy-start.8 = (f32[128]{0:T(128)S(1)}, f32[128]{0:T(128)}, u32[]{:S(2)}) copy-start(f32[128]{0:T(128)} %param.37) | copy-start | bytes 1540
  94.9 17.3 %copy-start.3 = (bf16[512,512]{1,0:T(8,128)(2,1)S(1)}, bf16[512,512]{1,0:T(8,128)(2,1)}, u32[]{:S(2)}) copy-start(bf16[512,512]{1,0:T(8,128)(2,1)} %param.39) | copy-start | bytes 1572868
  94.9 39.0 %copy-start.6 = (f32[2048]{0:T(1024)S(1)}, f32[2048]{0:T(1024)}, u32[]{:S(2)}) copy-start(f32[2048]{0:T(1024)} %param.40) | copy-start | bytes 24580
  95.7 1.3 copy-start.2
  113.0 60.4 %reduce-scatter.11.cloned.1.call-start = ((), (), s32[]{:S(2)}) async-start(), calls=%async_computation.7 | async-start | bytes 147456 | tf_op jit(solution)/shard_map/reduce_scatter | solution.py:153
Sparse Core Ops, SparseCore 0:
  30.7 31.5 reduce-scatter.4
  72.4 17.6 reduce-scatter.6
  113.1 5.6 reduce-scatter.8
  141.9 31.4 reduce-scatter.10
